TPU v7x, 512 devices: a 8x2x16 block of a 8x8x16 slice. The times are simulated.
512 devices in a mesh: grp: 2 (over y), sp: 32 (over z, core), tp: 8 (over x).
Axes of the slice: x: 8, y: 2, z: 16, core: 2. Of those that a mesh axis runs over, the one named last changes fastest.
The devices are a block of a 8x8x16 slice.
Arguments:
- out_gate: bfloat16 [24576, 1024], P(('grp', 'sp'), 'tp'), parts along dimension 0, may hold values from -6 to 6
- in_gate: bfloat16 [24576, 1024], P(('grp', 'sp'), 'tp'), parts along dimension 0, may hold values from -6 to 6
- conv_input: bfloat16 [24576, 1024], P(('grp', 'sp'), 'tp'), parts along dimension 0, may hold values from -6 to 6
- doc_ids: int32 [24576], P(('grp', 'sp')), parts along dimension 0, may hold values from 0 to 15, never falling along the last dimension, each value on 1 to 1536 neighbouring positions
- residual: bfloat16 [24576, 2048], P(('grp', 'sp'), 'tp'), parts along dimension 0, may hold values from -6 to 6
- conv_taps: float32 [3, 1024], P(None, 'tp'), may hold values from -6 to 6
- mix_gain: float32 [1024], P('tp'), may hold values from 0.1 to 1.9
- out_weight: bfloat16 [1024, 2048], P('tp'), may hold values from -0.1875 to 0.1875
- ffn_gain: float32 [2048], P('tp'), may hold values from 0.1 to 1.9
- routing: int32 [24576, 2], P(('grp', 'sp')), parts along dimension 0, may hold values from 0 to 63, as said below
- route_weight: float32 [24576, 2], P(('grp', 'sp')), parts along dimension 0, may hold values from 0.2 to 1.2
- expert_gate: bfloat16 [64, 2048, 512], P('sp', None, 'tp'), may hold values from -0.125 to 0.125
- expert_up: bfloat16 [64, 2048, 512], P('sp', None, 'tp'), may hold values from -0.125 to 0.125
- expert_down: bfloat16 [64, 512, 2048], P('sp', None, 'tp'), may hold values from -0.25 to 0.25
- shared_gate: bfloat16 [2048, 512], P(None, 'tp'), may hold values from -0.125 to 0.125
- shared_up: bfloat16 [2048, 512], P(None, 'tp'), may hold values from -0.125 to 0.125
- shared_down: bfloat16 [512, 2048], P(None, 'tp'), may hold values from -0.25 to 0.25
Outputs:
- layer_out: bfloat16 [24576, 2048], P(('grp', 'sp'), 'tp'), parts along dimension 0
There are 2 independent parts, one for each index of `grp`. A program takes and returns all parts, laid end to end along the dimension named above; an argument that names none is the same for every part. Nothing has to cross between parts.
Inputs may be any that keep to these rules, and one draw needn't show every extreme that they name: `routing`: each row names 2 different experts. In each aligned block of 48 rows no expert is named by more than 3 rows, and some expert is named by exactly 3 rows. `doc_ids`: never falls along the sequence; a document holds at most 1536 positions.
All inputs are finite; a program needn't handle non-finite values.
Results may differ from a plain program's by a relative error of at most 0.017.
Values may be sent and summed in bfloat16 or wider, within the bound.
No kernel may reach another device: no remote copies, remote signals or barrier semaphores. Data moves between devices by JAX's collectives and lax.ppermute only.
A program may use at most 64 MiB of HBM per device.

v0:
```python
import jax
import jax.numpy as jnp
from jax import lax
from jax.sharding import PartitionSpec as P

D_CONV = 1024
CONV_K = 3
TOPK = 2
EXP_DEV = 2


def from_behind(value, axis, steps):
    count = lax.axis_size(axis)
    first, last = (max(0, -steps), min(count, count - steps))
    return lax.ppermute(value, axis, [(source, source + steps) for source in range(first, last)])


def sent_to_all(shard, axis):
    copies = jnp.broadcast_to(shard, (lax.axis_size(axis), *shard.shape))
    return lax.all_to_all(copies, axis, split_axis=0, concat_axis=0, tiled=True)


def of_everyone(shard, axis):
    return sent_to_all(shard, axis).sum(axis=0)


def cut_along(shard, dim, length):
    shape = shard.shape
    pieces = shard.reshape(*shape[:dim], length, shape[dim] // length, *shape[dim + 1 :])
    return jnp.moveaxis(pieces, dim, 0)


def sum_at_owner(shard, axis, dim):
    pieces = cut_along(shard, dim, lax.axis_size(axis))
    arrived = lax.all_to_all(pieces, axis, split_axis=0, concat_axis=0, tiled=True)
    return arrived.astype(jnp.float32).sum(axis=0)


def rows_first(arrays, axis, dims):
    turned = [jnp.moveaxis(a, dim, 0) for a, dim in zip(arrays, dims)]
    both = jnp.concatenate([t.reshape(len(t), -1) for t in turned], axis=1)
    whole, at, finished = (lax.all_gather(both, axis, axis=0, tiled=True), 0, [])
    for t, dim in zip(turned, dims):
        slab = whole[:, at : at + t[0].size].reshape(-1, *t.shape[1:])
        finished.append(jnp.moveaxis(slab, 0, dim))
        at += t[0].size
    return tuple(finished)


def body(
    out_gate,
    in_gate,
    conv_input,
    doc_ids,
    residual,
    conv_taps,
    mix_gain,
    out_weight,
    ffn_gain,
    routing,
    route_weight,
    expert_gate,
    expert_up,
    expert_down,
    shared_gate,
    shared_up,
    shared_down,
):
    tokens = residual.shape[0]
    width = out_weight.shape[1]
    n_tp = lax.axis_size("tp")
    n_sp = lax.axis_size("sp")
    rows = tokens // n_tp
    experts = n_sp * EXP_DEV
    most = max(1, 2 * rows * TOPK // experts)
    slots = n_tp * most
    total = experts * slots
    cols = expert_down.shape[2]
    product = (in_gate.astype(jnp.float32) * conv_input.astype(jnp.float32)).astype(jnp.bfloat16)
    tail = (product[tokens - CONV_K + 1 :], doc_ids[tokens - CONV_K + 1 :].astype(jnp.bfloat16))
    prev_rows, prev_docs = from_behind((tail[0], tail[1]), "sp", 1)
    extended = jnp.concatenate([prev_rows, product], axis=0).astype(jnp.float32)
    ext_docs = jnp.concatenate([prev_docs.astype(jnp.int32), doc_ids])
    mixed = jnp.zeros(product.shape, jnp.float32)
    for k in range(CONV_K):
        keep = (ext_docs[k : k + tokens] == doc_ids)[:, None]
        mixed = mixed + jnp.where(keep, conv_taps[k] * extended[k : k + tokens], jnp.float32(0.0))
    conv_out = out_gate.astype(jnp.float32) * mixed
    squares = of_everyone(jnp.sum(conv_out * conv_out, axis=1), "tp")
    normed = (conv_out * lax.rsqrt(squares / D_CONV + 1e-06)[:, None] * mix_gain).astype(
        jnp.bfloat16
    )
    partial_value = jnp.dot(normed, out_weight, preferred_element_type=jnp.float32)
    proj = sum_at_owner(partial_value.astype(jnp.bfloat16), "tp", 1)
    stream = (residual.astype(jnp.float32) + proj).astype(jnp.bfloat16)
    stream32 = stream.astype(jnp.float32)
    stream_sq = of_everyone(jnp.sum(stream32 * stream32, axis=1), "tp")
    normal_cols = (stream32 * lax.rsqrt(stream_sq / width + 1e-06)[:, None] * ffn_gain).astype(
        jnp.bfloat16
    )
    flat_expert = routing.reshape(-1)
    onehot = (flat_expert[:, None] == jnp.arange(experts, dtype=jnp.int32)[None, :]).astype(
        jnp.int32
    )
    blocked = onehot.reshape(n_tp, rows * TOPK, experts)
    earlier = jnp.cumsum(blocked, axis=1) - blocked
    position = jnp.sum(earlier * blocked, axis=2).reshape(-1)
    entry = jnp.arange(tokens * TOPK, dtype=jnp.int32)
    slot = flat_expert * slots + entry // (rows * TOPK) * most + position
    table = jnp.full((total,), tokens, jnp.int32).at[slot].set(entry // TOPK)
    block_rows = lax.all_to_all(normal_cols, "tp", split_axis=0, concat_axis=1, tiled=True)
    mine = lax.dynamic_index_in_dim(
        table.reshape(n_sp, EXP_DEV, n_tp, most), lax.axis_index("tp"), 2, False
    )
    local = jnp.where(mine >= tokens, rows, mine - lax.axis_index("tp") * rows)
    padded_block = jnp.concatenate([block_rows, jnp.zeros((1, width), jnp.bfloat16)], axis=0)
    got = lax.all_to_all(padded_block[local], "sp", split_axis=0, concat_axis=0, tiled=True)
    arrived, whole = (
        lax.all_gather(got, "tp", axis=2, tiled=True),
        lax.all_gather(block_rows.reshape(1, 1, rows, width), "tp", axis=2, tiled=True),
    )
    normal = whole.reshape(tokens, width)
    gate = jnp.einsum("nesd,edh->nesh", arrived, expert_gate, preferred_element_type=jnp.float32)
    upper = jnp.einsum("nesd,edh->nesh", arrived, expert_up, preferred_element_type=jnp.float32)
    hidden = (jax.nn.silu(gate) * upper).astype(jnp.bfloat16)
    hidden_flat = hidden.reshape(n_sp * EXP_DEV * slots, hidden.shape[3])
    shared_hid = (
        jax.nn.silu(jnp.dot(normal, shared_gate, preferred_element_type=jnp.float32))
        * jnp.dot(normal, shared_up, preferred_element_type=jnp.float32)
    ).astype(jnp.bfloat16)
    expert_piece, shared_piece = rows_first((hidden_flat, shared_hid), "tp", (1, 1))
    count = expert_piece.shape[1]
    expert_part = jnp.einsum(
        "nesh,ehd->nesd",
        expert_piece.reshape(n_sp, EXP_DEV, slots, count),
        expert_down,
        preferred_element_type=jnp.float32,
    )
    shared_part = jnp.dot(shared_piece, shared_down, preferred_element_type=jnp.float32)
    returned = lax.all_to_all(
        expert_part.astype(jnp.bfloat16), "sp", split_axis=0, concat_axis=0, tiled=True
    )
    picked = (
        returned.reshape(total, cols)[slot].astype(jnp.float32) * route_weight.reshape(-1)[:, None]
    )
    routed = jnp.sum(picked.reshape(tokens, TOPK, cols), axis=1)
    return (stream32 + shared_part + routed).astype(jnp.bfloat16)


def solution(mesh):
    return jax.shard_map(
        body,
        mesh=mesh,
        in_specs=(
            P(("grp", "sp"), "tp"),
            P(("grp", "sp"), "tp"),
            P(("grp", "sp"), "tp"),
            P(("grp", "sp")),
            P(("grp", "sp"), "tp"),
            P(None, "tp"),
            P("tp"),
            P("tp", None),
            P("tp"),
            P(("grp", "sp"), None),
            P(("grp", "sp"), None),
            P("sp", None, "tp"),
            P("sp", None, "tp"),
            P("sp", None, "tp"),
            P(None, "tp"),
            P(None, "tp"),
            P(None, "tp"),
        ),
        out_specs=P(("grp", "sp"), "tp"),
        check_vma=False,
    )
```

profile of v0, /device:TPU:65, one launch (start us, length us, event | category | flops | bytes accessed | tf_op | source)
XLA Modules:
  0.0 412.4 jit_solution(5063214200456433942)
XLA Ops:
  6.6 1.0 multiply_convert_fusion.1
  7.6 7.1 %collective-permute-start.1 = (bf16[2,128]{1,0:T(2,128)(2,1)S(1)}, bf16[2,128]{1,0:T(2,128)(2,1)S(1)}, u32[]{:S(2)}, u32[]{:S(2)}) collective-permute-start(bf16[2,128]{1,0:T(2,128)(2,1)S(1)} %slice.53), channel_id=1, source_target_pairs={{0,8},{8,16},{16,24},{24,32},{32,40},{40,48},{48,56},{56,64},{64,7... | collective-permute-start | bytes 1544 | tf_op jit(solution)/shard_map/ppermute | solution.py:15
  14.7 0.7 convert.4
  15.4 1.9 collective-permute-start
  17.4 0.8 slice_bitcast_fusion.2
  18.2 34.9 %collective-permute-done = bf16[2]{0:T(256)(128)(2,1)S(1)} collective-permute-done((bf16[2]{0:T(256)(128)(2,1)S(1)}, bf16[2]{0:T(256)(128)(2,1)S(1)}, u32[]{:S(2)}, u32[]{:S(2)}) %collective-permute-start) | collective-permute-done | bytes 36 | tf_op jit(solution)/shard_map/ppermute | solution.py:15
  53.0 0.8 pad_add_fusion
  53.8 0.8 slice_compare_fusion.1
  54.6 1.2 multiply_reduce_fusion.1
  55.8 9.1 %all_to_all.46 = f32[8,1,384]{2,1,0:T(1,128)S(1)} all-to-all(f32[8,1,384]{2,1,0:T(1,128)S(1)} %broadcast_in_dim.50), channel_id=1, replica_groups=mesh['grp'=2,'sp'=32,'tp'=8] {'tp'}, dimensions={0} | all-to-all | bytes 24576 | tf_op jit(solution)/shard_map/all_to_all | solution.py:20
  64.9 0.6 convolution_convert_fusion
  65.5 1.3 copy.114
  66.8 3.9 all-to-all-start.1
  71.1 1.9 select_reduce_fusion
  73.5 35.1 %all-to-all-done.1 = bf16[8,384,256]{2,1,0:T(8,128)(2,1)S(1)} async-done(((bf16[8,384,256]{2,1,0:T(8,128)(2,1)}), bf16[8,384,256]{2,1,0:T(8,128)(2,1)S(1)}, u32[]{:S(2)}, u32[]{:S(2)}) %all-to-all-start.1) | async-done | bytes 1572896 | tf_op jit(solution)/shard_map/all_to_all | solution.py:35
  109.0 0.6 broadcast_in_dim.51
  109.6 3.7 all-to-all-start.2
  113.3 3.4 scatter_custom_fusion
  116.9 3.0 all-to-all-done.2
  120.0 0.8 fusion.51
  120.8 3.7 all-to-all-start.3
  124.7 8.5 %all-to-all-done.3 = bf16[8,48,256]{2,1,0:T(8,128)(2,1)S(1)} async-done(((bf16[8,48,256]{2,1,0:T(8,128)(2,1)}), bf16[8,48,256]{2,1,0:T(8,128)(2,1)S(1)}, u32[]{:S(2)}, u32[]{:S(2)}) %all-to-all-start.3) | async-done | bytes 196640 | tf_op jit(solution)/shard_map/all_to_all | solution.py:111
  133.2 1.1 gather_fusion
  134.3 0.5 reshape.189
  134.8 1.9 copy.75
  136.7 15.3 %all-to-all-start.4 = ((bf16[32,2,3,2048]{3,1,2,0:T(2,128)(2,1)}), bf16[32,2,3,2048]{3,1,2,0:T(2,128)(2,1)S(1)}, u32[]{:S(2)}, u32[]{:S(2)}) async-start(bf16[32,2,3,2048]{3,1,2,0:T(2,128)(2,1)} %copy.75), calls=%async_computation.4 | async-start | bytes 1572864 | tf_op jit(solution)/shard_map/all_to_all | solution.py:117
  152.2 0.8 reshape.183
  153.1 43.3 %all-to-all-done.4 = bf16[32,2,3,2048]{3,1,2,0:T(2,128)(2,1)S(1)} async-done(((bf16[32,2,3,2048]{3,1,2,0:T(2,128)(2,1)}), bf16[32,2,3,2048]{3,1,2,0:T(2,128)(2,1)S(1)}, u32[]{:S(2)}, u32[]{:S(2)}) %all-to-all-start.4) | async-done | bytes 786464 | tf_op jit(solution)/shard_map/all_to_all | solution.py:117
  196.4 1.2 copy.76
  197.7 0.2 all-gather.8.cloned.1.call-start
  198.0 2.1 fusion.30
  200.2 1.6 fusion.39
  201.9 76.6 %all-gather.4.cloned.1.call-done = bf16[32,2,24,2048]{3,0,1,2:T(8,128)(2,1)} async-done(((bf16[32,2,3,2048]{3,0,1,2:T(8,128)(2,1)}), bf16[32,2,24,2048]{3,0,1,2:T(8,128)(2,1)}) %all-gather.4.cloned.1.call-update) | async-done | bytes 6291472 | tf_op jit(solution)/shard_map/all_gather | solution.py:119
  278.6 4.7 %fusion.16 = f32[32,2,24,64]{3,0,2,1:T(8,128)S(1)} fusion(bf16[32,2,24,2048]{3,0,1,2:T(8,128)(2,1)} %all-gather.4.cloned.1.call-done, bf16[2,2048,64]{1,2,0:T(8,128)(2,1)S(1)} %copy-done.10), kind=kOutput, calls=%fused_computation.18 | convolution fusion | flops 402653184 | bytes 7208960 | tf_op jit(solution)/shard_map/nesd,edh->nesh/dot_general | solution.py:123
  283.3 1.8 fusion.25
  285.4 0.9 copy.82
  286.3 42.3 %all-gather.8.cloned.1.call-done = bf16[512,1920]{1,0:T(8,128)(2,1)} async-done(((bf16[64,1920]{1,0:T(8,128)(2,1)}), bf16[512,1920]{1,0:T(8,128)(2,1)}) %all-gather.8.cloned.1.call-update) | async-done | bytes 1966096 | tf_op jit(solution)/shard_map/all_gather | solution.py:42
  328.7 1.4 slice-done
  330.1 1.6 copy.92
  331.6 2.1 fusion.13
  333.7 1.0 copy.85
  334.7 18.1 %all-to-all-start.5 = ((bf16[32,2,24,256]{3,2,1,0:T(8,128)(2,1)}), bf16[32,2,24,256]{3,2,1,0:T(8,128)(2,1)S(1)}, u32[]{:S(2)}, u32[]{:S(2)}) async-start(bf16[32,2,24,256]{3,2,1,0:T(8,128)(2,1)} %copy.85), calls=%async_computation.5 | async-start | bytes 1572864 | tf_op jit(solution)/shard_map/all_to_all | solution.py:140
  352.8 0.8 copy.86
  353.6 43.6 %all-to-all-done.5 = bf16[32,2,24,256]{3,2,1,0:T(8,128)(2,1)S(1)} async-done(((bf16[32,2,24,256]{3,2,1,0:T(8,128)(2,1)}), bf16[32,2,24,256]{3,2,1,0:T(8,128)(2,1)S(1)}, u32[]{:S(2)}, u32[]{:S(2)}) %all-to-all-start.5) | async-done | bytes 786464 | tf_op jit(solution)/shard_map/all_to_all | solution.py:140
  397.2 3.3 gather_fusion.1
  400.4 1.5 reshape.187
  402.0 2.0 multiply_reduce_fusion
  403.9 1.9 fusion.29
  (65 shorter events, 2.7 us)
Async XLA Ops:
  6.5 58.3 %copy-start = (bf16[128,2048]{1,0:T(8,128)(2,1)S(1)}, bf16[128,2048]{1,0:T(8,128)(2,1)}, u32[]{:S(2)}) copy-start(bf16[128,2048]{1,0:T(8,128)(2,1)} %param.24) | copy-start | bytes 1572868
  6.6 58.3 %copy-start.8 = (f32[128]{0:T(128)S(1)}, f32[128]{0:T(128)}, u32[]{:S(2)}) copy-start(f32[128]{0:T(128)} %param.23) | copy-start | bytes 1540
  7.6 47.0 %collective-permute-start.1 = (bf16[2,128]{1,0:T(2,128)(2,1)S(1)}, bf16[2,128]{1,0:T(2,128)(2,1)S(1)}, u32[]{:S(2)}, u32[]{:S(2)}) collective-permute-start(bf16[2,128]{1,0:T(2,128)(2,1)S(1)} %slice.53), channel_id=1, source_target_pairs={{0,8},{8,16},{16,24},{24,32},{32,40},{40,48},{48,56},{56,64},{64,7... | collective-permute-start | bytes 1544 | tf_op jit(solution)/shard_map/ppermute | solution.py:15
  15.4 37.6 %collective-permute-start = (bf16[2]{0:T(256)(128)(2,1)S(1)}, bf16[2]{0:T(256)(128)(2,1)S(1)}, u32[]{:S(2)}, u32[]{:S(2)}) collective-permute-start(bf16[2]{0:T(256)(128)(2,1)S(1)} %slice.37), channel_id=1, source_target_pairs={{0,8},{8,16},{16,24},{24,32},{32,40},{40,48},{48,56},{56,64},{64,7... | collective-permute-start | bytes 20 | tf_op jit(solution)/shard_map/ppermute | solution.py:15
  66.8 3.9 copy-start.5
  66.8 41.9 %all-to-all-start.1 = ((bf16[8,384,256]{2,1,0:T(8,128)(2,1)}), bf16[8,384,256]{2,1,0:T(8,128)(2,1)S(1)}, u32[]{:S(2)}, u32[]{:S(2)}) async-start(bf16[8,384,256]{2,1,0:T(8,128)(2,1)} %bitcast.76), calls=%async_computation.1 | async-start | bytes 3145728 | tf_op jit(solution)/shard_map/all_to_all | solution.py:35
  70.7 38.2 %copy-start.4 = (bf16[384,256]{1,0:T(8,128)(2,1)S(1)}, bf16[384,256]{1,0:T(8,128)(2,1)}, u32[]{:S(2)}) copy-start(bf16[384,256]{1,0:T(8,128)(2,1)} %param.21) | copy-start | bytes 589828
  73.5 46.5 %copy-start.7 = (f32[256]{0:T(256)S(1)}, f32[256]{0:T(256)}, u32[]{:S(2)}) copy-start(f32[256]{0:T(256)} %param.25) | copy-start | bytes 3076
  109.6 10.3 %all-to-all-start.2 = ((f32[8,1,384]{2,1,0:T(1,128)}), f32[8,1,384]{2,1,0:T(1,128)S(1)}, u32[]{:S(2)}, u32[]{:S(2)}) async-start(f32[8,1,384]{2,1,0:T(1,128)} %broadcast_in_dim.51), calls=%async_computation.2 | async-start | bytes 24576 | tf_op jit(solution)/shard_map/all_to_all | solution.py:20
  120.8 12.4 %all-to-all-start.3 = ((bf16[8,48,256]{2,1,0:T(8,128)(2,1)}), bf16[8,48,256]{2,1,0:T(8,128)(2,1)S(1)}, u32[]{:S(2)}, u32[]{:S(2)}) async-start(bf16[8,48,256]{2,1,0:T(8,128)(2,1)} %bitcast.4), calls=%async_computation.3 | async-start | bytes 393216 | tf_op jit(solution)/shard_map/all_to_all | solution.py:111
  136.7 59.7 %all-to-all-start.4 = ((bf16[32,2,3,2048]{3,1,2,0:T(2,128)(2,1)}), bf16[32,2,3,2048]{3,1,2,0:T(2,128)(2,1)S(1)}, u32[]{:S(2)}, u32[]{:S(2)}) async-start(bf16[32,2,3,2048]{3,1,2,0:T(2,128)(2,1)} %copy.75), calls=%async_computation.4 | async-start | bytes 1572864 | tf_op jit(solution)/shard_map/all_to_all | solution.py:117
  152.0 46.0 %all-gather.6.cloned.1.call-start = ((), (), s32[]{:S(2)}) async-start(), calls=%async_computation.7 | async-start | bytes 1769472 | tf_op jit(solution)/shard_map/all_gather | solution.py:120
  152.2 45.8 %copy-start.3 = (bf16[2048,64]{0,1:T(8,128)(2,1)S(1)}, bf16[2048,64]{0,1:T(8,128)(2,1)}, u32[]{:S(2)}) copy-start(bf16[2048,64]{0,1:T(8,128)(2,1)} %param.31) | copy-start | bytes 786436
  153.0 125.6 %all-gather.4.cloned.1.call-start = ((), (), s32[]{:S(2)}) async-start(), calls=%async_computation.6 | async-start | bytes 7077888 | tf_op jit(solution)/shard_map/all_gather | solution.py:119
  197.7 130.9 %all-gather.8.cloned.1.call-start = ((), (), s32[]{:S(2)}) async-start(), calls=%async_computation.8 | async-start | bytes 2211840 | tf_op jit(solution)/shard_map/all_gather | solution.py:42
  198.0 2.1 copy-start.2
  200.2 78.4 %copy-start.10 = (bf16[2,2048,64]{1,2,0:T(8,128)(2,1)S(1)}, bf16[2,2048,64]{1,2,0:T(8,128)(2,1)}, u32[]{:S(2)}) copy-start(bf16[2,2048,64]{1,2,0:T(8,128)(2,1)} %param.28) | copy-start | bytes 1572868
  201.9 81.4 %copy-start.11 = (bf16[2,2048,64]{1,2,0:T(8,128)(2,1)S(1)}, bf16[2,2048,64]{1,2,0:T(8,128)(2,1)}, u32[]{:S(2)}) copy-start(bf16[2,2048,64]{1,2,0:T(8,128)(2,1)} %param.29) | copy-start | bytes 1572868
  278.6 4.7 %copy-start.9 = (bf16[32,2,24,2048]{3,0,1,2:T(8,128)(2,1)S(1)}, bf16[32,2,24,2048]{3,0,1,2:T(8,128)(2,1)}, u32[]{:S(2)}) copy-start(bf16[32,2,24,2048]{3,0,1,2:T(8,128)(2,1)} %all-gather.4.cloned.1.call-done) | copy-start | bytes 18874372
  328.6 1.4 slice-start
  333.7 19.0 %copy-start.6 = (f32[384,2]{0,1:T(2,128)S(1)}, f32[384,2]{0,1:T(2,128)}, u32[]{:S(2)}) copy-start(f32[384,2]{0,1:T(2,128)} %param.27) | copy-start | bytes 9220
  334.7 62.5 %all-to-all-start.5 = ((bf16[32,2,24,256]{3,2,1,0:T(8,128)(2,1)}), bf16[32,2,24,256]{3,2,1,0:T(8,128)(2,1)S(1)}, u32[]{:S(2)}, u32[]{:S(2)}) async-start(bf16[32,2,24,256]{3,2,1,0:T(8,128)(2,1)} %copy.85), calls=%async_computation.5 | async-start | bytes 1572864 | tf_op jit(solution)/shard_map/all_to_all | solution.py:140
  400.4 3.5 copy-start.1
Sparse Core Ops, SparseCore 0:
  154.9 37.8 all-gather.5
  197.8 80.6 all-gather.3
  286.5 42.1 all-gather.7
where the time goes:
time: 413 us; the launch traced here: 412 us
  waiting for transfers between devices  287 us (69%)
  starting transfers between devices  54 us (13%)
  local copies, waits for them, and re-layouts  23.7 us (6%)
  matrix products  14.9 us (4%)
  between operations  13.6 us (3%)
  other arithmetic  9.74 us (2%)
  blocking collectives  9.06 us (2%)
    all_gather x1, waiting for transfers between devices, body(): lax.all_gather(got, 'tp', axis=2, tiled=True)  76.6 us
    all_to_all x1, waiting for transfers between devices, body(): lax.all_to_all(expert_part.astype(jnp.bfloat16), 'sp', split_axis=0, conc...  43.6 us
    all_to_all x1, waiting for transfers between devices, body(): lax.all_to_all(padded_block[local], 'sp', split_axis=0, concat_axis=0, ti...  43.3 us
    all_gather x1, waiting for transfers between devices, rows_first(): lax.all_gather(both, axis, axis=0, tiled=True)  42.3 us
    all_to_all x1, waiting for transfers between devices, sum_at_owner(): lax.all_to_all(pieces, axis, split_axis=0, concat_axis=0, tiled=True)  35.1 us
    ppermute x2, waiting for transfers between devices, from_behind(): lax.ppermute(value, axis, [(source, source + steps) for source in range(f...  34.9 us
    all_to_all x1, starting transfers between devices, body(): lax.all_to_all(expert_part.astype(jnp.bfloat16), 'sp', split_axis=0, conc...  18.1 us
    all_to_all x1, starting transfers between devices, body(): lax.all_to_all(padded_block[local], 'sp', split_axis=0, concat_axis=0, ti...  15.3 us
  transfers between devices with their start and end apart: 10, of which 8 were waited for; matrix products, arithmetic and copies ran while one was open for 4% of the time, Pallas kernels for 0%

commit v1 on v0

--- a/solution.py
+++ b/solution.py
@@ -115,8 +115,21 @@
     local = jnp.where(mine >= tokens, rows, mine - lax.axis_index("tp") * rows)
     padded_block = jnp.concatenate([block_rows, jnp.zeros((1, width), jnp.bfloat16)], axis=0)
     got = lax.all_to_all(padded_block[local], "sp", split_axis=0, concat_axis=0, tiled=True)
+
+    def meet_loops(m, row_axis, dim_no):
+        m_next = jnp.concatenate(
+            lax.all_to_all(
+                jnp.stack([m] * lax.axis_size(row_axis)),
+                split_axis=0,
+                concat_axis=0,
+                axis_name=row_axis,
+            ),
+            axis=dim_no,
+        )
+        return m_next
+
     arrived, whole = (
-        lax.all_gather(got, "tp", axis=2, tiled=True),
+        meet_loops(got, "tp", 2),
         lax.all_gather(block_rows.reshape(1, 1, rows, width), "tp", axis=2, tiled=True),
     )
     normal = whole.reshape(tokens, width)

time: 413 us -> 484 us (1.17)
  blocking collectives: 9.06 us -> 68.6 us
  waiting for transfers between devices: 287 us -> 307 us
  starting transfers between devices: 54 us -> 43.7 us
  local copies, waits for them, and re-layouts: 23.7 us -> 28.7 us
    all_gather x1 -> x0, waiting for transfers between devices: 76.6 us -> none  [body(): lax.all_gather(got, 'tp', axis=2, tiled=True)]
    all_gather x1, waiting for transfers between devices: 0.02 us -> 75.1 us  [body(): lax.all_gather(block_rows.reshape(1, 1, rows, width), 'tp', axis=2, tiled...]
    all_to_all x0 -> x1, blocking collectives: none -> 59.5 us  [body(): lax.all_to_all(padded_block[local], 'sp', split_axis=0, concat_axis=0, ti...]
    all_to_all x1, waiting for transfers between devices: 43.3 us -> 77.1 us  [meet_loops(): lax.all_to_all(jnp.stack([m] * lax.axis_size(row_axis)), split_axis=0, co...]
    all_gather x1, waiting for transfers between devices: 42.3 us -> 30 us  [rows_first(): lax.all_gather(both, axis, axis=0, tiled=True)]
    all_to_all x1, starting transfers between devices: 15.3 us -> 5.06 us  [meet_loops(): lax.all_to_all(jnp.stack([m] * lax.axis_size(row_axis)), split_axis=0, co...]
  transfers between devices with their start and end apart: 10 -> 9, of which waited for: 8 -> 8; matrix products, arithmetic and copies ran while one was open for 4% -> 3% of each run, Pallas kernels for 0% -> 0%
where the time goes in v1:
time: 484 us; the launch traced here: 483 us
  waiting for transfers between devices  307 us (63%)
  blocking collectives  68.6 us (14%)
  starting transfers between devices  43.7 us (9%)
  local copies, waits for them, and re-layouts  28.7 us (6%)
  between operations  13.9 us (3%)
  matrix products  10.8 us (2%)
  other arithmetic  9.74 us (2%)
    all_to_all x1, waiting for transfers between devices, meet_loops(): lax.all_to_all(jnp.stack([m] * lax.axis_size(row_axis)), split_axis=0, co...  77.1 us
    all_gather x1, waiting for transfers between devices, body(): lax.all_gather(block_rows.reshape(1, 1, rows, width), 'tp', axis=2, tiled...  75.1 us
    all_to_all x1, blocking collectives, body(): lax.all_to_all(padded_block[local], 'sp', split_axis=0, concat_axis=0, ti...  59.5 us
    all_to_all x1, waiting for transfers between devices, body(): lax.all_to_all(expert_part.astype(jnp.bfloat16), 'sp', split_axis=0, conc...  43.6 us
    all_to_all x1, waiting for transfers between devices, sum_at_owner(): lax.all_to_all(pieces, axis, split_axis=0, concat_axis=0, tiled=True)  35.1 us
    ppermute x2, waiting for transfers between devices, from_behind(): lax.ppermute(value, axis, [(source, source + steps) for source in range(f...  34.9 us
    all_gather x1, waiting for transfers between devices, rows_first(): lax.all_gather(both, axis, axis=0, tiled=True)  30 us
    all_to_all x1, starting transfers between devices, body(): lax.all_to_all(expert_part.astype(jnp.bfloat16), 'sp', split_axis=0, conc...  18.1 us
  transfers between devices with their start and end apart: 9, of which 8 were waited for; matrix products, arithmetic and copies ran while one was open for 3% of the time, Pallas kernels for 0%

profile of v1, /device:TPU:65, one launch (start us, length us, event | category | flops | bytes accessed | tf_op | source)
XLA Modules:
  0.0 482.7 jit_solution(10616251995891030938)
XLA Ops:
  6.6 1.0 multiply_convert_fusion.1
  7.6 7.1 %collective-permute-start.1 = (bf16[2,128]{1,0:T(2,128)(2,1)S(1)}, bf16[2,128]{1,0:T(2,128)(2,1)S(1)}, u32[]{:S(2)}, u32[]{:S(2)}) collective-permute-start(bf16[2,128]{1,0:T(2,128)(2,1)S(1)} %slice.53), channel_id=1, source_target_pairs={{0,8},{8,16},{16,24},{24,32},{32,40},{40,48},{48,56},{56,64},{64,7... | collective-permute-start | bytes 1544 | tf_op jit(solution)/shard_map/ppermute | solution.py:15
  14.7 0.7 convert.4
  15.4 1.9 collective-permute-start
  17.4 0.8 slice_bitcast_fusion.2
  18.2 34.9 %collective-permute-done = bf16[2]{0:T(256)(128)(2,1)S(1)} collective-permute-done((bf16[2]{0:T(256)(128)(2,1)S(1)}, bf16[2]{0:T(256)(128)(2,1)S(1)}, u32[]{:S(2)}, u32[]{:S(2)}) %collective-permute-start) | collective-permute-done | bytes 36 | tf_op jit(solution)/shard_map/ppermute | solution.py:15
  53.0 0.8 pad_add_fusion
  53.8 0.8 slice_compare_fusion.1
  54.6 1.2 multiply_reduce_fusion.1
  55.8 9.1 %all_to_all.51 = f32[8,1,384]{2,1,0:T(1,128)S(1)} all-to-all(f32[8,1,384]{2,1,0:T(1,128)S(1)} %broadcast_in_dim.50), channel_id=1, replica_groups=mesh['grp'=2,'sp'=32,'tp'=8] {'tp'}, dimensions={0} | all-to-all | bytes 24576 | tf_op jit(solution)/shard_map/all_to_all | solution.py:20
  64.9 0.6 convolution_convert_fusion
  65.5 1.3 copy.102
  66.7 3.9 all-to-all-start.1
  71.1 1.9 select_reduce_fusion
  73.5 35.1 %all-to-all-done.1 = bf16[8,384,256]{2,1,0:T(8,128)(2,1)S(1)} async-done(((bf16[8,384,256]{2,1,0:T(8,128)(2,1)}), bf16[8,384,256]{2,1,0:T(8,128)(2,1)S(1)}, u32[]{:S(2)}, u32[]{:S(2)}) %all-to-all-start.1) | async-done | bytes 1572896 | tf_op jit(solution)/shard_map/all_to_all | solution.py:35
  109.0 0.6 broadcast_in_dim.51
  109.6 3.7 all-to-all-start.2
  113.3 3.4 scatter_custom_fusion
  116.9 3.0 all-to-all-done.2
  120.0 0.8 fusion.37
  120.8 3.7 all-to-all-start.3
  124.7 8.5 %all-to-all-done.3 = bf16[8,48,256]{2,1,0:T(8,128)(2,1)S(1)} async-done(((bf16[8,48,256]{2,1,0:T(8,128)(2,1)}), bf16[8,48,256]{2,1,0:T(8,128)(2,1)S(1)}, u32[]{:S(2)}, u32[]{:S(2)}) %all-to-all-start.3) | async-done | bytes 196640 | tf_op jit(solution)/shard_map/all_to_all | solution.py:111
  133.2 1.1 gather_fusion
  134.8 1.0 copy.76
  135.8 59.5 %all_to_all.52 = bf16[32,2,3,2048]{3,1,2,0:T(2,128)(2,1)S(1)} all-to-all(bf16[32,2,3,2048]{3,1,2,0:T(2,128)(2,1)S(1)} %copy.76), channel_id=1, replica_groups=mesh['grp'=2,'sp'=32,'tp'=8] {'sp'}, dimensions={0} | all-to-all | bytes 1572864 | tf_op jit(solution)/shard_map/all_to_all | solution.py:117
  195.6 3.5 stack.2
  199.1 5.1 %all-to-all-start.5 = ((bf16[8,32,2,3,2048]{4,1,3,2,0:T(8,128)(2,1)}), bf16[8,32,2,3,2048]{4,1,3,2,0:T(8,128)(2,1)}, u32[]{:S(2)}, u32[]{:S(2)}) async-start(bf16[8,32,2,3,2048]{4,1,3,2,0:T(8,128)(2,1)} %stack.2), calls=%async_computation.5 | async-start | bytes 12582912 | tf_op jit(solution)/shard_map/all_to_all | solution.py:121
  204.3 0.8 reshape.193
  205.4 75.1 %all-gather.3.cloned.1.call-done = bf16[1,1,384,2048]{3,2,1,0:T(8,128)(2,1)} async-done(((bf16[1,1,48,2048]{3,2,1,0:T(8,128)(2,1)}), bf16[1,1,384,2048]{3,2,1,0:T(8,128)(2,1)}) %all-gather.3.cloned.1.call-update) | async-done | bytes 1572880 | tf_op jit(solution)/shard_map/all_gather | solution.py:133
  280.4 2.1 fusion.16
  282.6 0.6 fusion.25
  283.3 77.1 %all-to-all-done.5 = bf16[8,32,2,3,2048]{4,1,3,2,0:T(8,128)(2,1)} async-done(((bf16[8,32,2,3,2048]{4,1,3,2,0:T(8,128)(2,1)}), bf16[8,32,2,3,2048]{4,1,3,2,0:T(8,128)(2,1)}, u32[]{:S(2)}, u32[]{:S(2)}) %all-to-all-start.5) | async-done | bytes 6291488 | tf_op jit(solution)/shard_map/all_to_all | solution.py:121
  360.5 3.4 copy.78
  363.9 1.8 convolution_bitcast_fusion.1
  365.6 1.8 fusion.13
  367.7 0.9 copy.82
  368.7 30.0 %all-gather.5.cloned.1.call-done = bf16[512,1920]{1,0:T(8,128)(2,1)} async-done(((bf16[64,1920]{1,0:T(8,128)(2,1)}), bf16[512,1920]{1,0:T(8,128)(2,1)}) %all-gather.5.cloned.1.call-update) | async-done | bytes 1966096 | tf_op jit(solution)/shard_map/all_gather | solution.py:42
  398.7 1.4 slice-done
  400.1 1.6 copy.92
  401.7 2.0 fusion.9
  403.7 1.0 copy.85
  404.7 18.1 %all-to-all-start.6 = ((bf16[32,2,24,256]{3,2,1,0:T(8,128)(2,1)}), bf16[32,2,24,256]{3,2,1,0:T(8,128)(2,1)S(1)}, u32[]{:S(2)}, u32[]{:S(2)}) async-start(bf16[32,2,24,256]{3,2,1,0:T(8,128)(2,1)} %copy.85), calls=%async_computation.6 | async-start | bytes 1572864 | tf_op jit(solution)/shard_map/all_to_all | solution.py:153
  422.7 0.8 copy.86
  423.6 43.6 %all-to-all-done.6 = bf16[32,2,24,256]{3,2,1,0:T(8,128)(2,1)S(1)} async-done(((bf16[32,2,24,256]{3,2,1,0:T(8,128)(2,1)}), bf16[32,2,24,256]{3,2,1,0:T(8,128)(2,1)S(1)}, u32[]{:S(2)}, u32[]{:S(2)}) %all-to-all-start.6) | async-done | bytes 786464 | tf_op jit(solution)/shard_map/all_to_all | solution.py:153
  467.1 3.3 gather_fusion.1
  470.4 1.5 reshape.197
  471.9 2.0 multiply_reduce_fusion
  473.9 1.9 fusion.15
  (67 shorter events, 3.5 us)
Async XLA Ops:
  6.5 58.3 %copy-start = (bf16[128,2048]{1,0:T(8,128)(2,1)S(1)}, bf16[128,2048]{1,0:T(8,128)(2,1)}, u32[]{:S(2)}) copy-start(bf16[128,2048]{1,0:T(8,128)(2,1)} %param.24) | copy-start | bytes 1572868
  6.6 58.3 %copy-start.9 = (f32[128]{0:T(128)S(1)}, f32[128]{0:T(128)}, u32[]{:S(2)}) copy-start(f32[128]{0:T(128)} %param.23) | copy-start | bytes 1540
  7.6 47.0 %collective-permute-start.1 = (bf16[2,128]{1,0:T(2,128)(2,1)S(1)}, bf16[2,128]{1,0:T(2,128)(2,1)S(1)}, u32[]{:S(2)}, u32[]{:S(2)}) collective-permute-start(bf16[2,128]{1,0:T(2,128)(2,1)S(1)} %slice.53), channel_id=1, source_target_pairs={{0,8},{8,16},{16,24},{24,32},{32,40},{40,48},{48,56},{56,64},{64,7... | collective-permute-start | bytes 1544 | tf_op jit(solution)/shard_map/ppermute | solution.py:15
  15.4 37.6 %collective-permute-start = (bf16[2]{0:T(256)(128)(2,1)S(1)}, bf16[2]{0:T(256)(128)(2,1)S(1)}, u32[]{:S(2)}, u32[]{:S(2)}) collective-permute-start(bf16[2]{0:T(256)(128)(2,1)S(1)} %slice.37), channel_id=1, source_target_pairs={{0,8},{8,16},{16,24},{24,32},{32,40},{40,48},{48,56},{56,64},{64,7... | collective-permute-start | bytes 20 | tf_op jit(solution)/shard_map/ppermute | solution.py:15
  66.7 3.9 copy-start.6
  66.7 41.9 %all-to-all-start.1 = ((bf16[8,384,256]{2,1,0:T(8,128)(2,1)}), bf16[8,384,256]{2,1,0:T(8,128)(2,1)S(1)}, u32[]{:S(2)}, u32[]{:S(2)}) async-start(bf16[8,384,256]{2,1,0:T(8,128)(2,1)} %bitcast.81), calls=%async_computation.1 | async-start | bytes 3145728 | tf_op jit(solution)/shard_map/all_to_all | solution.py:35
  70.7 38.2 %copy-start.5 = (bf16[384,256]{1,0:T(8,128)(2,1)S(1)}, bf16[384,256]{1,0:T(8,128)(2,1)}, u32[]{:S(2)}) copy-start(bf16[384,256]{1,0:T(8,128)(2,1)} %param.21) | copy-start | bytes 589828
  73.5 46.5 %copy-start.8 = (f32[256]{0:T(256)S(1)}, f32[256]{0:T(256)}, u32[]{:S(2)}) copy-start(f32[256]{0:T(256)} %param.25) | copy-start | bytes 3076
  109.6 10.3 %all-to-all-start.2 = ((f32[8,1,384]{2,1,0:T(1,128)}), f32[8,1,384]{2,1,0:T(1,128)S(1)}, u32[]{:S(2)}, u32[]{:S(2)}) async-start(f32[8,1,384]{2,1,0:T(1,128)} %broadcast_in_dim.51), calls=%async_computation.2 | async-start | bytes 24576 | tf_op jit(solution)/shard_map/all_to_all | solution.py:20
  120.8 12.4 %all-to-all-start.3 = ((bf16[8,48,256]{2,1,0:T(8,128)(2,1)}), bf16[8,48,256]{2,1,0:T(8,128)(2,1)S(1)}, u32[]{:S(2)}, u32[]{:S(2)}) async-start(bf16[8,48,256]{2,1,0:T(8,128)(2,1)} %bitcast.4), calls=%async_computation.3 | async-start | bytes 393216 | tf_op jit(solution)/shard_map/all_to_all | solution.py:111
  199.1 81.4 %copy-start.4 = (bf16[2048,64]{0,1:T(8,128)(2,1)S(1)}, bf16[2048,64]{0,1:T(8,128)(2,1)}, u32[]{:S(2)}) copy-start(bf16[2048,64]{0,1:T(8,128)(2,1)} %param.31) | copy-start | bytes 786436
  199.1 161.4 %all-to-all-start.5 = ((bf16[8,32,2,3,2048]{4,1,3,2,0:T(8,128)(2,1)}), bf16[8,32,2,3,2048]{4,1,3,2,0:T(8,128)(2,1)}, u32[]{:S(2)}, u32[]{:S(2)}) async-start(bf16[8,32,2,3,2048]{4,1,3,2,0:T(8,128)(2,1)} %stack.2), calls=%async_computation.5 | async-start | bytes 12582912 | tf_op jit(solution)/shard_map/all_to_all | solution.py:121
  204.1 78.5 %copy-start.12 = (bf16[2048,64]{0,1:T(8,128)(2,1)S(1)}, bf16[2048,64]{0,1:T(8,128)(2,1)}, u32[]{:S(2)}) copy-start(bf16[2048,64]{0,1:T(8,128)(2,1)} %param.32) | copy-start | bytes 786436
  204.1 76.3 %all-gather.3.cloned.1.call-start = ((), (), s32[]{:S(2)}) async-start(), calls=%async_computation.7 | async-start | bytes 1769472 | tf_op jit(solution)/shard_map/all_gather | solution.py:133
  205.1 193.6 %all-gather.5.cloned.1.call-start = ((), (), s32[]{:S(2)}) async-start(), calls=%async_computation.8 | async-start | bytes 2211840 | tf_op jit(solution)/shard_map/all_gather | solution.py:42
  280.4 2.1 copy-start.2
  283.3 80.5 %copy-start.3 = (bf16[2,2048,64]{1,2,0:T(8,128)(2,1)S(1)}, bf16[2,2048,64]{1,2,0:T(8,128)(2,1)}, u32[]{:S(2)}) copy-start(bf16[2,2048,64]{1,2,0:T(8,128)(2,1)} %param.28) | copy-start | bytes 1572868
  363.8 1.8 copy-start.10
  398.7 1.4 slice-start
  400.1 1.6 copy-start.11
  403.7 19.1 %copy-start.7 = (f32[384,2]{0,1:T(2,128)S(1)}, f32[384,2]{0,1:T(2,128)}, u32[]{:S(2)}) copy-start(f32[384,2]{0,1:T(2,128)} %param.27) | copy-start | bytes 9220
  404.7 62.5 %all-to-all-start.6 = ((bf16[32,2,24,256]{3,2,1,0:T(8,128)(2,1)}), bf16[32,2,24,256]{3,2,1,0:T(8,128)(2,1)S(1)}, u32[]{:S(2)}, u32[]{:S(2)}) async-start(bf16[32,2,24,256]{3,2,1,0:T(8,128)(2,1)} %copy.85), calls=%async_computation.6 | async-start | bytes 1572864 | tf_op jit(solution)/shard_map/all_to_all | solution.py:153
  470.4 3.5 copy-start.1
Sparse Core Ops, SparseCore 0:
  207.1 73.3 all-gather.2
  368.8 29.8 all-gather.4
